TPU v7x, 32 devices: a whole 2x2x4 slice. The times are simulated.
32 devices in a mesh: sp: 4 (over y, x), tp: 8 (over z, core).
Axes of the slice: x: 2, y: 2, z: 4, core: 2. Of those that a mesh axis runs over, the one named last changes fastest.
Arguments:
- stream: bfloat16 [4096, 1024], P('tp', 'sp'), may hold values from -6 to 6
- value_weight: bfloat16 [2, 2048, 4096], P(None, 'tp', 'sp'), may hold values from -0.09375 to 0.09375
- gate_weight: bfloat16 [2, 2048, 4096], P(None, 'tp', 'sp'), may hold values from -0.09375 to 0.09375
- conv_taps: bfloat16 [2, 2048, 31], P(None, 'tp'), may hold values from -16 to 16
- norm_gain: bfloat16 [2, 2048], P(None, 'tp'), may hold values from 0.099609375 to 1.8984375
- out_weight: bfloat16 [2, 4096, 2048], P(None, 'tp', 'sp'), may hold values from -4 to 4
- out_gain: bfloat16 [2, 4096], P(None, 'tp'), may hold values from 0.099609375 to 1.8984375
Outputs:
- result: bfloat16 [4096, 1024], P('tp', 'sp')
All inputs are finite; a program needn't handle non-finite values.
Results may differ from a plain program's by a relative error of at most 0.015.
Values may be sent and summed in bfloat16 or wider, within the bound.
A program may use at most 64 MiB of HBM per device.

v0:
```python
import jax
import jax.numpy as jnp
from jax import lax
from jax.sharding import PartitionSpec as P

D = 4096
W = 2048
LAYERS = 2


def with_halo(cells, sides, width):
    for axis, dim in sides:
        count = lax.axis_size(axis)
        ends = count - 1
        head = lax.slice_in_dim(cells, 0, width, axis=dim)
        tail = lax.slice_in_dim(cells, cells.shape[dim] - width, cells.shape[dim], axis=dim)
        cells = jnp.concatenate(
            [
                lax.ppermute(tail, axis, [(i, (i + 1) % count) for i in range(ends)]),
                cells,
                lax.ppermute(head, axis, [((i + 1) % count, i) for i in range(ends)]),
            ],
            axis=dim,
        )
    return cells


def finish_layer(hidden, branch, feature_gain):
    branch_wide = lax.optimization_barrier(branch.astype(jnp.bfloat16)).astype(jnp.float32)
    square_total = lax.psum(jnp.sum(branch_wide * branch_wide, axis=0), "tp")
    factor = lax.rsqrt(square_total / D + 1e-06)
    return (hidden.astype(jnp.float32) + branch_wide * factor * feature_gain).astype(jnp.bfloat16)


def on_device(stream, value_weight, gate_weight, conv_taps, norm_gain, out_weight, out_gain):
    hidden = stream
    positions = hidden.shape[1]
    for layer_index in range(LAYERS):
        value_cols, gate_cols, out_cols = (
            lax.all_gather(value_weight[layer_index], "sp", axis=1, tiled=True),
            lax.all_gather(gate_weight[layer_index], "sp", axis=1, tiled=True),
            lax.all_gather(out_weight[layer_index], "sp", axis=1, tiled=True),
        )
        block_rows = lax.all_gather(hidden, "tp", axis=0, tiled=True)
        value_proj = jnp.dot(value_cols, block_rows, preferred_element_type=jnp.float32)
        gate_proj = jnp.dot(gate_cols, block_rows, preferred_element_type=jnp.float32)
        gated = (value_proj * jax.nn.sigmoid(gate_proj)).astype(jnp.bfloat16)
        kernel_taps = conv_taps[layer_index].astype(jnp.float32)
        reach = kernel_taps.shape[1] // 2
        padded = with_halo(gated, (("sp", 1),), reach).astype(jnp.float32)
        convolved = jnp.zeros(gated.shape, jnp.float32)
        for offset in range(kernel_taps.shape[1]):
            convolved = (
                convolved
                + kernel_taps[:, offset : offset + 1] * padded[:, offset : offset + positions]
            )
        conv_narrow = lax.optimization_barrier(convolved.astype(jnp.bfloat16))
        feature_gain = out_gain[layer_index].astype(jnp.float32)[:, None]
        conv_wide = conv_narrow.astype(jnp.float32)
        channel_totals = lax.psum(
            (jnp.sum(conv_wide, axis=0), jnp.sum(conv_wide * conv_wide, axis=0)), "tp"
        )
        average = channel_totals[0] / W
        variance = channel_totals[1] / W - average * average
        channel_gain = norm_gain[layer_index].astype(jnp.float32)[:, None]
        activated = jax.nn.silu(
            (conv_wide - average) * lax.rsqrt(variance + 1e-05) * channel_gain
        ).astype(jnp.bfloat16)
        branch = jnp.dot(
            out_cols,
            lax.all_gather(activated, "tp", axis=0, tiled=True),
            preferred_element_type=jnp.float32,
        )
        hidden = finish_layer(hidden, branch, feature_gain)
    return hidden


def solution(mesh):
    return jax.shard_map(
        on_device,
        mesh=mesh,
        in_specs=(
            P("tp", "sp"),
            P(None, "tp", "sp"),
            P(None, "tp", "sp"),
            P(None, "tp", None),
            P(None, "tp"),
            P(None, "tp", "sp"),
            P(None, "tp"),
        ),
        out_specs=P("tp", "sp"),
        check_vma=False,
    )
```

profile of v0, /device:TPU:0, one launch (start us, length us, event | category | flops | bytes accessed | tf_op | source)
XLA Modules:
  0.0 368.0 jit_solution(12427185381842521671)
XLA Ops:
  6.5 2.4 fusion.155
  8.9 0.0 all-gather.27.cloned.1.call-update
  8.9 0.0 all-gather.17.cloned.1.call-start
  9.0 0.7 all-gather.17.cloned.1.call-update
  9.7 0.0 all-gather.25.cloned.1.call-start
  9.7 1.0 fusion.154
  10.8 0.0 all-gather.25.cloned.1.call-update
  10.8 0.0 all-gather.29.cloned.1.call-start
  10.8 1.1 fusion.153
  11.9 0.0 all-gather.29.cloned.1.call-update
  11.9 0.0 all-gather.19.cloned.1.call-start
  12.1 35.0 %all-gather.27.cloned.1.call-done = bf16[1,256,4096]{2,1,0:T(8,128)(2,1)} async-done(((bf16[1,256,1024]{2,1,0:T(8,128)(2,1)}), bf16[1,256,4096]{2,1,0:T(8,128)(2,1)}) %all-gather.27.cloned.1.call-update) | async-done | bytes 2097168 | tf_op jit(solution)/shard_map/all_gather | solution.py:41
  47.1 30.8 %all-gather.17.cloned.1.call-done = bf16[4096,256]{1,0:T(8,128)(2,1)} async-done(((bf16[512,256]{1,0:T(8,128)(2,1)}), bf16[4096,256]{1,0:T(8,128)(2,1)}) %all-gather.17.cloned.1.call-update) | async-done | bytes 2097168 | tf_op jit(solution)/shard_map/all_gather | solution.py:44
  77.9 3.3 fusion.36
  81.2 0.0 copy-start.8
  81.2 33.1 %all-gather.25.cloned.1.call-done = bf16[1,256,4096]{2,1,0:T(8,128)(2,1)} async-done(((bf16[1,256,1024]{2,1,0:T(8,128)(2,1)}), bf16[1,256,4096]{2,1,0:T(8,128)(2,1)}) %all-gather.25.cloned.1.call-update) | async-done | bytes 2097168 | tf_op jit(solution)/shard_map/all_gather | solution.py:40
  114.4 2.5 fusion.57
  116.9 1.3 collective-permute-start.1
  118.2 4.5 %collective-permute-start = (bf16[256,15]{0,1:T(8,128)(2,1)S(1)}, bf16[256,15]{0,1:T(8,128)(2,1)S(1)}, u32[]{:S(2)}, u32[]{:S(2)}) collective-permute-start(bf16[256,15]{0,1:T(8,128)(2,1)S(1)} %get-tuple-element.21), channel_id=1, source_target_pairs={{0,8},{8,16},{16,24},{1,9},{9,17},{17,25},{2,10},{10,18},{18,26},{... | collective-permute-start | bytes 23048 | tf_op jit(solution)/shard_map/ppermute | solution.py:19
  122.8 1.3 collective-permute-done
  124.1 0.0 copy-start.5
  124.1 0.0 copy-start.7
  124.2 0.7 fusion.121
  124.8 0.1 convert_reduce_fusion.1
  125.0 15.1 %all-reduce.1 = (f32[256]{0:T(256)S(1)}, f32[256]{0:T(256)S(1)}) all-reduce(f32[256]{0:T(256)S(1)} %get-tuple-element.8, f32[256]{0:T(256)S(1)} %get-tuple-element.7), channel_id=1, replica_groups=mesh['sp'=4,'tp'=8] {'tp'}, use_global_device_ids=true, to_apply=%region_3.0 | all-reduce | flops 512 | bytes 4096 | tf_op jit(solution)/shard_map/psum | solution.py:60
  140.1 0.8 fusion.78
  140.9 0.0 all-gather.19.cloned.1.call-update
  140.9 0.0 all-gather.33.cloned.1.call-start
  141.0 0.5 all-gather.33.cloned.1.call-update
  141.5 0.0 all-gather.21.cloned.1.call-start
  141.6 0.1 copy.12
  141.7 9.4 %all-gather.29.cloned.1.call-done = bf16[1,512,2048]{2,1,0:T(8,128)(2,1)} async-done(((bf16[1,512,512]{2,1,0:T(8,128)(2,1)}), bf16[1,512,2048]{2,1,0:T(8,128)(2,1)}) %all-gather.29.cloned.1.call-update) | async-done | bytes 2097168 | tf_op jit(solution)/shard_map/all_gather | solution.py:42
  151.1 25.3 %all-gather.19.cloned.1.call-done = bf16[2048,256]{0,1:T(8,128)(2,1)} async-done(((bf16[256,256]{0,1:T(8,128)(2,1)}), bf16[2048,256]{0,1:T(8,128)(2,1)}) %all-gather.19.cloned.1.call-update) | async-done | bytes 1048592 | tf_op jit(solution)/shard_map/all_gather | solution.py:71
  176.5 2.7 fusion.21
  179.1 0.1 fusion.63
  179.3 15.7 %psum.44 = f32[256]{0:T(256)S(1)} all-reduce(f32[256]{0:T(256)S(1)} %fusion.63), channel_id=1, replica_groups=mesh['sp'=4,'tp'=8] {'tp'}, use_global_device_ids=true, to_apply=%region_5.6 | all-reduce | flops 256 | bytes 2048 | tf_op jit(solution)/shard_map/psum | solution.py:30
  195.0 0.9 fusion.66
  195.9 0.0 all-gather.21.cloned.1.call-update
  195.9 0.0 all-gather.31.cloned.1.call-start
  196.0 0.7 all-gather.31.cloned.1.call-update
  196.7 0.0 all-gather.35.cloned.1.call-start
  196.7 0.7 all-gather.35.cloned.1.call-update
  197.4 0.0 all-gather.23.cloned.1.call-start
  197.5 14.7 %all-gather.33.cloned.1.call-done = bf16[1,256,4096]{2,1,0:T(8,128)(2,1)} async-done(((bf16[1,256,1024]{2,1,0:T(8,128)(2,1)}), bf16[1,256,4096]{2,1,0:T(8,128)(2,1)}) %all-gather.33.cloned.1.call-update) | async-done | bytes 2097168 | tf_op jit(solution)/shard_map/all_gather | solution.py:41
  212.1 30.8 %all-gather.21.cloned.1.call-done = bf16[4096,256]{0,1:T(8,128)(2,1)} async-done(((bf16[512,256]{0,1:T(8,128)(2,1)}), bf16[4096,256]{0,1:T(8,128)(2,1)}) %all-gather.21.cloned.1.call-update) | async-done | bytes 2097168 | tf_op jit(solution)/shard_map/all_gather | solution.py:44
  242.9 3.1 fusion.51
  246.0 33.3 %all-gather.31.cloned.1.call-done = bf16[1,256,4096]{2,1,0:T(8,128)(2,1)} async-done(((bf16[1,256,1024]{2,1,0:T(8,128)(2,1)}), bf16[1,256,4096]{2,1,0:T(8,128)(2,1)}) %all-gather.31.cloned.1.call-update) | async-done | bytes 2097168 | tf_op jit(solution)/shard_map/all_gather | solution.py:40
  279.4 2.3 fusion.60
  281.7 1.3 collective-permute-start.3
  283.0 4.5 %collective-permute-start.2 = (bf16[256,15]{0,1:T(8,128)(2,1)S(1)}, bf16[256,15]{0,1:T(8,128)(2,1)S(1)}, u32[]{:S(2)}, u32[]{:S(2)}) collective-permute-start(bf16[256,15]{0,1:T(8,128)(2,1)S(1)} %get-tuple-element.19), channel_id=1, source_target_pairs={{0,8},{8,16},{16,24},{1,9},{9,17},{17,25},{2,10},{10,18},{18,26},{... | collective-permute-start | bytes 23048 | tf_op jit(solution)/shard_map/ppermute | solution.py:19
  287.6 0.0 collective-permute-done.3
  287.6 1.3 collective-permute-done.2
  289.0 0.7 fusion.90
  289.6 0.1 convert_reduce_fusion
  289.8 15.1 %all-reduce = (f32[256]{0:T(256)S(1)}, f32[256]{0:T(256)S(1)}) all-reduce(f32[256]{0:T(256)S(1)} %get-tuple-element.6, f32[256]{0:T(256)S(1)} %get-tuple-element.5), channel_id=1, replica_groups=mesh['sp'=4,'tp'=8] {'tp'}, use_global_device_ids=true, to_apply=%region_9.10 | all-reduce | flops 512 | bytes 4096 | tf_op jit(solution)/shard_map/psum | solution.py:60
  304.9 0.8 fusion.87
  305.7 0.0 all-gather.23.cloned.1.call-update
  305.7 10.5 %all-gather.35.cloned.1.call-done = bf16[1,512,2048]{2,1,0:T(8,128)(2,1)} async-done(((bf16[1,512,512]{2,1,0:T(8,128)(2,1)}), bf16[1,512,2048]{2,1,0:T(8,128)(2,1)}) %all-gather.35.cloned.1.call-update) | async-done | bytes 2097168 | tf_op jit(solution)/shard_map/all_gather | solution.py:42
  316.3 25.3 %all-gather.23.cloned.1.call-done = bf16[2048,256]{0,1:T(8,128)(2,1)} async-done(((bf16[256,256]{0,1:T(8,128)(2,1)}), bf16[2048,256]{0,1:T(8,128)(2,1)}) %all-gather.23.cloned.1.call-update) | async-done | bytes 1048592 | tf_op jit(solution)/shard_map/all_gather | solution.py:71
  341.6 2.7 fusion.18
  344.3 0.1 fusion.67
  344.4 15.7 %psum.47 = f32[256]{0:T(256)S(1)} all-reduce(f32[256]{0:T(256)S(1)} %fusion.67), channel_id=1, replica_groups=mesh['sp'=4,'tp'=8] {'tp'}, use_global_device_ids=true, to_apply=%region_11.12 | all-reduce | flops 256 | bytes 2048 | tf_op jit(solution)/shard_map/psum | solution.py:30
  360.2 0.2 fusion.70
  360.4 0.8 copy.17
  (33 shorter events, 0.3 us)
Async XLA Ops:
  6.5 3.2 copy-start.3
  6.5 40.6 %all-gather.27.cloned.1.call-start = ((), (), s32[]{:S(2)}) async-start(), calls=%async_computation.5 | async-start | bytes 2621440 | tf_op jit(solution)/shard_map/all_gather | solution.py:41
  8.9 1.9 copy-start.4
  8.9 69.0 %all-gather.17.cloned.1.call-start = ((), (), s32[]{:S(2)}) async-start(), calls=%async_computation | async-start | bytes 2359296 | tf_op jit(solution)/shard_map/all_gather | solution.py:44
  9.7 104.7 %all-gather.25.cloned.1.call-start = ((), (), s32[]{:S(2)}) async-start(), calls=%async_computation.4 | async-start | bytes 2621440 | tf_op jit(solution)/shard_map/all_gather | solution.py:40
  10.8 1.2 copy-start.6
  10.8 140.3 %all-gather.29.cloned.1.call-start = ((), (), s32[]{:S(2)}) async-start(), calls=%async_computation.6 | async-start | bytes 2621440 | tf_op jit(solution)/shard_map/all_gather | solution.py:42
  11.9 164.5 %all-gather.19.cloned.1.call-start = ((), (), s32[]{:S(2)}) async-start(), calls=%async_computation.1 | async-start | bytes 1179648 | tf_op jit(solution)/shard_map/all_gather | solution.py:71
  77.9 36.5 %copy-start.1 = (bf16[4096,256]{1,0:T(8,128)(2,1)S(1)}, bf16[4096,256]{1,0:T(8,128)(2,1)}, u32[]{:S(2)}) copy-start(bf16[4096,256]{1,0:T(8,128)(2,1)} %all-gather.17.cloned.1.call-done) | copy-start | bytes 6291460
  81.2 41.5 %copy-start.8 = (bf16[2,256]{1,0:T(2,128)(2,1)S(1)}, bf16[2,256]{1,0:T(2,128)(2,1)}, u32[]{:S(2)}) copy-start(bf16[2,256]{1,0:T(2,128)(2,1)} %param.11) | copy-start | bytes 3076
  116.9 5.9 %collective-permute-start.1 = (bf16[256,15]{0,1:T(8,128)(2,1)S(1)}, bf16[256,15]{0,1:T(8,128)(2,1)S(1)}, u32[]{:S(2)}, u32[]{:S(2)}) collective-permute-start(bf16[256,15]{0,1:T(8,128)(2,1)S(1)} %get-tuple-element.22), channel_id=1, source_target_pairs={{8,0},{16,8},{24,16},{9,1},{17,9},{25,17},{10,2},{18,10},{26,18},{... | collective-permute-start | bytes 23048 | tf_op jit(solution)/shard_map/ppermute | solution.py:21
  118.2 5.9 %collective-permute-start = (bf16[256,15]{0,1:T(8,128)(2,1)S(1)}, bf16[256,15]{0,1:T(8,128)(2,1)S(1)}, u32[]{:S(2)}, u32[]{:S(2)}) collective-permute-start(bf16[256,15]{0,1:T(8,128)(2,1)S(1)} %get-tuple-element.21), channel_id=1, source_target_pairs={{0,8},{8,16},{16,24},{1,9},{9,17},{17,25},{2,10},{10,18},{18,26},{... | collective-permute-start | bytes 23048 | tf_op jit(solution)/shard_map/ppermute | solution.py:19
  124.1 17.4 %copy-start.5 = (bf16[512,256]{1,0:T(8,128)(2,1)S(1)}, bf16[512,256]{1,0:T(8,128)(2,1)}, u32[]{:S(2)}) copy-start(bf16[512,256]{1,0:T(8,128)(2,1)} %param.7) | copy-start | bytes 786436
  124.1 17.6 %copy-start.7 = (bf16[2,512]{1,0:T(2,128)(2,1)S(1)}, bf16[2,512]{1,0:T(2,128)(2,1)}, u32[]{:S(2)}) copy-start(bf16[2,512]{1,0:T(2,128)(2,1)} %param.13) | copy-start | bytes 6148
  140.9 71.2 %all-gather.33.cloned.1.call-start = ((), (), s32[]{:S(2)}) async-start(), calls=%async_computation.8 | async-start | bytes 2621440 | tf_op jit(solution)/shard_map/all_gather | solution.py:41
  141.5 101.4 %all-gather.21.cloned.1.call-start = ((), (), s32[]{:S(2)}) async-start(), calls=%async_computation.2 | async-start | bytes 2359296 | tf_op jit(solution)/shard_map/all_gather | solution.py:44
  195.9 83.4 %all-gather.31.cloned.1.call-start = ((), (), s32[]{:S(2)}) async-start(), calls=%async_computation.7 | async-start | bytes 2621440 | tf_op jit(solution)/shard_map/all_gather | solution.py:40
  196.7 119.6 %all-gather.35.cloned.1.call-start = ((), (), s32[]{:S(2)}) async-start(), calls=%async_computation.9 | async-start | bytes 2621440 | tf_op jit(solution)/shard_map/all_gather | solution.py:42
  197.4 144.2 %all-gather.23.cloned.1.call-start = ((), (), s32[]{:S(2)}) async-start(), calls=%async_computation.3 | async-start | bytes 1179648 | tf_op jit(solution)/shard_map/all_gather | solution.py:71
  242.9 36.5 %copy-start.2 = (bf16[4096,256]{0,1:T(8,128)(2,1)S(1)}, bf16[4096,256]{0,1:T(8,128)(2,1)}, u32[]{:S(2)}) copy-start(bf16[4096,256]{0,1:T(8,128)(2,1)} %all-gather.21.cloned.1.call-done) | copy-start | bytes 6291460
  281.7 5.9 %collective-permute-start.3 = (bf16[256,15]{0,1:T(8,128)(2,1)S(1)}, bf16[256,15]{0,1:T(8,128)(2,1)S(1)}, u32[]{:S(2)}, u32[]{:S(2)}) collective-permute-start(bf16[256,15]{0,1:T(8,128)(2,1)S(1)} %get-tuple-element.20), channel_id=1, source_target_pairs={{8,0},{16,8},{24,16},{9,1},{17,9},{25,17},{10,2},{18,10},{26,18},{... | collective-permute-start | bytes 23048 | tf_op jit(solution)/shard_map/ppermute | solution.py:21
  283.0 5.9 %collective-permute-start.2 = (bf16[256,15]{0,1:T(8,128)(2,1)S(1)}, bf16[256,15]{0,1:T(8,128)(2,1)S(1)}, u32[]{:S(2)}, u32[]{:S(2)}) collective-permute-start(bf16[256,15]{0,1:T(8,128)(2,1)S(1)} %get-tuple-element.19), channel_id=1, source_target_pairs={{0,8},{8,16},{16,24},{1,9},{9,17},{17,25},{2,10},{10,18},{18,26},{... | collective-permute-start | bytes 23048 | tf_op jit(solution)/shard_map/ppermute | solution.py:19
  305.7 54.5 %copy-start = (bf16[512,256]{0,1:T(8,128)(2,1)S(1)}, bf16[512,256]{0,1:T(8,128)(2,1)}, u32[]{:S(2)}) copy-start(bf16[512,256]{0,1:T(8,128)(2,1)} %fusion.66) | copy-start | bytes 786436
Sparse Core Ops, SparseCore 0:
  9.2 37.8 all-gather.26
  48.7 29.1 all-gather.16
  79.7 34.5 all-gather.24
  116.0 35.0 all-gather.28
  152.5 23.8 all-gather.18
  178.2 33.9 all-gather.32
  213.7 29.1 all-gather.20
  244.8 34.5 all-gather.30
  281.2 35.0 all-gather.34
  317.7 23.8 all-gather.22
where the time goes:
time: 368 us
  waiting for transfers between devices  254 us (69%)
  blocking collectives  61.6 us (17%)
  matrix products  16.6 us (5%)
  between operations  13.8 us (4%)
  starting transfers between devices  12 us (3%)
  local copies, waits for them, and re-layouts  5.6 us (2%)
  other arithmetic  4.78 us (1%)
    all_gather x2, waiting for transfers between devices, on_device(): lax.all_gather(value_weight[layer_index], 'sp', axis=1, tiled=True)  66.4 us
    all_gather x2, waiting for transfers between devices, on_device(): block_rows = lax.all_gather(hidden, 'tp', axis=0, tiled=True)  61.6 us
    all_gather x2, waiting for transfers between devices, on_device(): lax.all_gather(activated, 'tp', axis=0, tiled=True)  50.7 us
    all_gather x2, waiting for transfers between devices, on_device(): lax.all_gather(gate_weight[layer_index], 'sp', axis=1, tiled=True)  49.7 us
    psum x2, blocking collectives, finish_layer(): square_total = lax.psum(jnp.sum(branch_wide * branch_wide, axis=0), 'tp')  31.5 us
    psum x2, blocking collectives, on_device(): lax.psum((jnp.sum(conv_wide, axis=0), jnp.sum(conv_wide * conv_wide, axis...  30.1 us
    all_gather x2, waiting for transfers between devices, on_device(): lax.all_gather(out_weight[layer_index], 'sp', axis=1, tiled=True)  19.9 us
    ppermute x2, starting transfers between devices, with_halo(): lax.ppermute(tail, axis, [(i, (i + 1) % count) for i in range(ends)])  9.09 us
  transfers between devices with their start and end apart: 14, of which 12 were waited for; matrix products, arithmetic and copies ran while one was open for 6% of the time, Pallas kernels for 0%

commit v1 on v0

--- a/solution.py
+++ b/solution.py
@@ -27,7 +27,7 @@
 
 def finish_layer(hidden, branch, feature_gain):
     branch_wide = lax.optimization_barrier(branch.astype(jnp.bfloat16)).astype(jnp.float32)
-    square_total = lax.psum(jnp.sum(branch_wide * branch_wide, axis=0), "tp")
+    square_total = jnp.sum(lax.all_gather(jnp.sum(branch_wide * branch_wide, axis=0), "tp"), axis=0)
     factor = lax.rsqrt(square_total / D + 1e-06)
     return (hidden.astype(jnp.float32) + branch_wide * factor * feature_gain).astype(jnp.bfloat16)
 

time: 368 us -> 363 us (0.986)
  blocking collectives: 61.6 us -> 51.6 us
  waiting for transfers between devices: 254 us -> 259 us
    psum x2 -> x0, blocking collectives: 31.5 us -> none  [finish_layer(): square_total = lax.psum(jnp.sum(branch_wide * branch_wide, axis=0), 'tp')]
    all_gather x0 -> x2, blocking collectives: none -> 21.5 us  [finish_layer(): lax.all_gather(jnp.sum(branch_wide * branch_wide, axis=0), 'tp')]
    all_gather x2, waiting for transfers between devices: 49.7 us -> 54.6 us  [on_device(): lax.all_gather(gate_weight[layer_index], 'sp', axis=1, tiled=True)]
where the time goes in v1:
time: 363 us
  waiting for transfers between devices  259 us (71%)
  blocking collectives  51.6 us (14%)
  matrix products  16.6 us (5%)
  between operations  13.8 us (4%)
  starting transfers between devices  12 us (3%)
  local copies, waits for them, and re-layouts  5.6 us (2%)
  other arithmetic  4.84 us (1%)
    all_gather x2, waiting for transfers between devices, on_device(): lax.all_gather(value_weight[layer_index], 'sp', axis=1, tiled=True)  66.4 us
    all_gather x2, waiting for transfers between devices, on_device(): block_rows = lax.all_gather(hidden, 'tp', axis=0, tiled=True)  61.6 us
    all_gather x2, waiting for transfers between devices, on_device(): lax.all_gather(gate_weight[layer_index], 'sp', axis=1, tiled=True)  54.6 us
    all_gather x2, waiting for transfers between devices, on_device(): lax.all_gather(activated, 'tp', axis=0, tiled=True)  50.7 us
    psum x2, blocking collectives, on_device(): lax.psum((jnp.sum(conv_wide, axis=0), jnp.sum(conv_wide * conv_wide, axis...  30.1 us
    all_gather x2, blocking collectives, finish_layer(): lax.all_gather(jnp.sum(branch_wide * branch_wide, axis=0), 'tp')  21.5 us
    all_gather x2, waiting for transfers between devices, on_device(): lax.all_gather(out_weight[layer_index], 'sp', axis=1, tiled=True)  19.9 us
    ppermute x2, starting transfers between devices, with_halo(): lax.ppermute(tail, axis, [(i, (i + 1) % count) for i in range(ends)])  9.09 us
  transfers between devices with their start and end apart: 14, of which 12 were waited for; matrix products, arithmetic and copies ran while one was open for 6% of the time, Pallas kernels for 0%

profile of v1, /device:TPU:0, one launch (start us, length us, event | category | flops | bytes accessed | tf_op | source)
XLA Modules:
  0.0 363.0 jit_solution(18314734911827368086)
XLA Ops:
  6.5 2.4 fusion.155
  8.9 0.0 all-gather.31.cloned.1.call-update
  8.9 0.0 all-gather.21.cloned.1.call-start
  9.0 0.7 all-gather.21.cloned.1.call-update
  9.7 0.0 all-gather.29.cloned.1.call-start
  9.7 1.0 fusion.154
  10.8 0.0 all-gather.29.cloned.1.call-update
  10.8 0.0 all-gather.33.cloned.1.call-start
  10.8 1.1 fusion.153
  11.9 0.0 all-gather.33.cloned.1.call-update
  11.9 0.0 all-gather.23.cloned.1.call-start
  12.1 35.0 %all-gather.31.cloned.1.call-done = bf16[1,256,4096]{2,1,0:T(8,128)(2,1)} async-done(((bf16[1,256,1024]{2,1,0:T(8,128)(2,1)}), bf16[1,256,4096]{2,1,0:T(8,128)(2,1)}) %all-gather.31.cloned.1.call-update) | async-done | bytes 2097168 | tf_op jit(solution)/shard_map/all_gather | solution.py:41
  47.1 30.8 %all-gather.21.cloned.1.call-done = bf16[4096,256]{1,0:T(8,128)(2,1)} async-done(((bf16[512,256]{1,0:T(8,128)(2,1)}), bf16[4096,256]{1,0:T(8,128)(2,1)}) %all-gather.21.cloned.1.call-update) | async-done | bytes 2097168 | tf_op jit(solution)/shard_map/all_gather | solution.py:44
  77.9 3.3 fusion.36
  81.2 0.0 copy-start.8
  81.2 33.1 %all-gather.29.cloned.1.call-done = bf16[1,256,4096]{2,1,0:T(8,128)(2,1)} async-done(((bf16[1,256,1024]{2,1,0:T(8,128)(2,1)}), bf16[1,256,4096]{2,1,0:T(8,128)(2,1)}) %all-gather.29.cloned.1.call-update) | async-done | bytes 2097168 | tf_op jit(solution)/shard_map/all_gather | solution.py:40
  114.4 2.5 fusion.57
  116.9 1.3 collective-permute-start.1
  118.2 4.5 %collective-permute-start = (bf16[256,15]{0,1:T(8,128)(2,1)S(1)}, bf16[256,15]{0,1:T(8,128)(2,1)S(1)}, u32[]{:S(2)}, u32[]{:S(2)}) collective-permute-start(bf16[256,15]{0,1:T(8,128)(2,1)S(1)} %get-tuple-element.21), channel_id=1, source_target_pairs={{0,8},{8,16},{16,24},{1,9},{9,17},{17,25},{2,10},{10,18},{18,26},{... | collective-permute-start | bytes 23048 | tf_op jit(solution)/shard_map/ppermute | solution.py:19
  122.8 0.0 collective-permute-done.1
  122.8 1.3 collective-permute-done
  124.1 0.0 copy-start.5
  124.1 0.0 copy-start.7
  124.2 0.7 fusion.121
  124.8 0.1 convert_reduce_fusion.1
  125.0 15.1 %all-reduce.1 = (f32[256]{0:T(256)S(1)}, f32[256]{0:T(256)S(1)}) all-reduce(f32[256]{0:T(256)S(1)} %get-tuple-element.8, f32[256]{0:T(256)S(1)} %get-tuple-element.7), channel_id=1, replica_groups=mesh['sp'=4,'tp'=8] {'tp'}, use_global_device_ids=true, to_apply=%region_3.0 | all-reduce | flops 512 | bytes 4096 | tf_op jit(solution)/shard_map/psum | solution.py:60
  140.1 0.8 fusion.78
  140.9 0.0 all-gather.23.cloned.1.call-update
  140.9 0.0 all-gather.37.cloned.1.call-start
  141.0 0.5 all-gather.37.cloned.1.call-update
  141.5 0.0 all-gather.25.cloned.1.call-start
  141.6 0.1 copy.18
  141.7 9.4 %all-gather.33.cloned.1.call-done = bf16[1,512,2048]{2,1,0:T(8,128)(2,1)} async-done(((bf16[1,512,512]{2,1,0:T(8,128)(2,1)}), bf16[1,512,2048]{2,1,0:T(8,128)(2,1)}) %all-gather.33.cloned.1.call-update) | async-done | bytes 2097168 | tf_op jit(solution)/shard_map/all_gather | solution.py:42
  151.1 25.3 %all-gather.23.cloned.1.call-done = bf16[2048,256]{0,1:T(8,128)(2,1)} async-done(((bf16[256,256]{0,1:T(8,128)(2,1)}), bf16[2048,256]{0,1:T(8,128)(2,1)}) %all-gather.23.cloned.1.call-update) | async-done | bytes 1048592 | tf_op jit(solution)/shard_map/all_gather | solution.py:71
  176.5 2.7 fusion.21
  179.1 0.1 fusion.63
  179.3 10.7 %all-gather.8 = f32[8,1,256]{2,1,0:T(1,128)S(1)} all-gather(f32[1,1,256]{2,1,0:T(1,128)S(1)} %bitcast.144), channel_id=5, replica_groups=mesh['sp'=4,'tp'=8] {'tp'}, dimensions={0}, use_global_device_ids=true | all-gather | bytes 9216 | tf_op jit(solution)/shard_map/all_gather | solution.py:30
  190.0 0.9 fusion.66
  190.9 0.0 all-gather.25.cloned.1.call-update
  190.9 0.0 all-gather.35.cloned.1.call-start
  191.0 0.7 all-gather.35.cloned.1.call-update
  191.7 0.0 all-gather.39.cloned.1.call-start
  191.7 0.7 all-gather.39.cloned.1.call-update
  192.4 0.0 all-gather.27.cloned.1.call-start
  192.5 19.6 %all-gather.37.cloned.1.call-done = bf16[1,256,4096]{2,1,0:T(8,128)(2,1)} async-done(((bf16[1,256,1024]{2,1,0:T(8,128)(2,1)}), bf16[1,256,4096]{2,1,0:T(8,128)(2,1)}) %all-gather.37.cloned.1.call-update) | async-done | bytes 2097168 | tf_op jit(solution)/shard_map/all_gather | solution.py:41
  212.1 30.8 %all-gather.25.cloned.1.call-done = bf16[4096,256]{0,1:T(8,128)(2,1)} async-done(((bf16[512,256]{0,1:T(8,128)(2,1)}), bf16[4096,256]{0,1:T(8,128)(2,1)}) %all-gather.25.cloned.1.call-update) | async-done | bytes 2097168 | tf_op jit(solution)/shard_map/all_gather | solution.py:44
  242.9 3.1 fusion.51
  246.0 33.3 %all-gather.35.cloned.1.call-done = bf16[1,256,4096]{2,1,0:T(8,128)(2,1)} async-done(((bf16[1,256,1024]{2,1,0:T(8,128)(2,1)}), bf16[1,256,4096]{2,1,0:T(8,128)(2,1)}) %all-gather.35.cloned.1.call-update) | async-done | bytes 2097168 | tf_op jit(solution)/shard_map/all_gather | solution.py:40
  279.4 2.3 fusion.60
  281.7 1.3 collective-permute-start.3
  283.0 4.5 %collective-permute-start.2 = (bf16[256,15]{0,1:T(8,128)(2,1)S(1)}, bf16[256,15]{0,1:T(8,128)(2,1)S(1)}, u32[]{:S(2)}, u32[]{:S(2)}) collective-permute-start(bf16[256,15]{0,1:T(8,128)(2,1)S(1)} %get-tuple-element.19), channel_id=1, source_target_pairs={{0,8},{8,16},{16,24},{1,9},{9,17},{17,25},{2,10},{10,18},{18,26},{... | collective-permute-start | bytes 23048 | tf_op jit(solution)/shard_map/ppermute | solution.py:19
  287.6 1.3 collective-permute-done.2
  288.9 0.7 fusion.90
  289.6 0.1 convert_reduce_fusion
  289.8 15.1 %all-reduce = (f32[256]{0:T(256)S(1)}, f32[256]{0:T(256)S(1)}) all-reduce(f32[256]{0:T(256)S(1)} %get-tuple-element.6, f32[256]{0:T(256)S(1)} %get-tuple-element.5), channel_id=1, replica_groups=mesh['sp'=4,'tp'=8] {'tp'}, use_global_device_ids=true, to_apply=%region_9.10 | all-reduce | flops 512 | bytes 4096 | tf_op jit(solution)/shard_map/psum | solution.py:60
  304.9 0.8 fusion.87
  305.7 0.0 all-gather.27.cloned.1.call-update
  305.7 10.5 %all-gather.39.cloned.1.call-done = bf16[1,512,2048]{2,1,0:T(8,128)(2,1)} async-done(((bf16[1,512,512]{2,1,0:T(8,128)(2,1)}), bf16[1,512,2048]{2,1,0:T(8,128)(2,1)}) %all-gather.39.cloned.1.call-update) | async-done | bytes 2097168 | tf_op jit(solution)/shard_map/all_gather | solution.py:42
  316.3 25.3 %all-gather.27.cloned.1.call-done = bf16[2048,256]{0,1:T(8,128)(2,1)} async-done(((bf16[256,256]{0,1:T(8,128)(2,1)}), bf16[2048,256]{0,1:T(8,128)(2,1)}) %all-gather.27.cloned.1.call-update) | async-done | bytes 1048592 | tf_op jit(solution)/shard_map/all_gather | solution.py:71
  341.6 2.7 fusion.18
  344.3 0.1 fusion.67
  344.4 10.7 %all-gather.9 = f32[8,1,256]{2,1,0:T(1,128)S(1)} all-gather(f32[1,1,256]{2,1,0:T(1,128)S(1)} %bitcast.145), channel_id=9, replica_groups=mesh['sp'=4,'tp'=8] {'tp'}, dimensions={0}, use_global_device_ids=true | all-gather | bytes 9216 | tf_op jit(solution)/shard_map/all_gather | solution.py:30
  355.2 0.2 fusion.70
  355.4 0.8 copy.23
  (35 shorter events, 0.3 us)
Async XLA Ops:
  6.5 3.2 copy-start.3
  6.5 40.6 %all-gather.31.cloned.1.call-start = ((), (), s32[]{:S(2)}) async-start(), calls=%async_computation.5 | async-start | bytes 2621440 | tf_op jit(solution)/shard_map/all_gather | solution.py:41
  8.9 1.9 copy-start.4
  8.9 69.0 %all-gather.21.cloned.1.call-start = ((), (), s32[]{:S(2)}) async-start(), calls=%async_computation | async-start | bytes 2359296 | tf_op jit(solution)/shard_map/all_gather | solution.py:44
  9.7 104.7 %all-gather.29.cloned.1.call-start = ((), (), s32[]{:S(2)}) async-start(), calls=%async_computation.4 | async-start | bytes 2621440 | tf_op jit(solution)/shard_map/all_gather | solution.py:40
  10.8 1.2 copy-start.6
  10.8 140.3 %all-gather.33.cloned.1.call-start = ((), (), s32[]{:S(2)}) async-start(), calls=%async_computation.6 | async-start | bytes 2621440 | tf_op jit(solution)/shard_map/all_gather | solution.py:42
  11.9 164.5 %all-gather.23.cloned.1.call-start = ((), (), s32[]{:S(2)}) async-start(), calls=%async_computation.1 | async-start | bytes 1179648 | tf_op jit(solution)/shard_map/all_gather | solution.py:71
  77.9 36.5 %copy-start.1 = (bf16[4096,256]{1,0:T(8,128)(2,1)S(1)}, bf16[4096,256]{1,0:T(8,128)(2,1)}, u32[]{:S(2)}) copy-start(bf16[4096,256]{1,0:T(8,128)(2,1)} %all-gather.21.cloned.1.call-done) | copy-start | bytes 6291460
  81.2 41.5 %copy-start.8 = (bf16[2,256]{1,0:T(2,128)(2,1)S(1)}, bf16[2,256]{1,0:T(2,128)(2,1)}, u32[]{:S(2)}) copy-start(bf16[2,256]{1,0:T(2,128)(2,1)} %param.11) | copy-start | bytes 3076
  116.9 5.9 %collective-permute-start.1 = (bf16[256,15]{0,1:T(8,128)(2,1)S(1)}, bf16[256,15]{0,1:T(8,128)(2,1)S(1)}, u32[]{:S(2)}, u32[]{:S(2)}) collective-permute-start(bf16[256,15]{0,1:T(8,128)(2,1)S(1)} %get-tuple-element.22), channel_id=1, source_target_pairs={{8,0},{16,8},{24,16},{9,1},{17,9},{25,17},{10,2},{18,10},{26,18},{... | collective-permute-start | bytes 23048 | tf_op jit(solution)/shard_map/ppermute | solution.py:21
  118.2 5.9 %collective-permute-start = (bf16[256,15]{0,1:T(8,128)(2,1)S(1)}, bf16[256,15]{0,1:T(8,128)(2,1)S(1)}, u32[]{:S(2)}, u32[]{:S(2)}) collective-permute-start(bf16[256,15]{0,1:T(8,128)(2,1)S(1)} %get-tuple-element.21), channel_id=1, source_target_pairs={{0,8},{8,16},{16,24},{1,9},{9,17},{17,25},{2,10},{10,18},{18,26},{... | collective-permute-start | bytes 23048 | tf_op jit(solution)/shard_map/ppermute | solution.py:19
  124.1 17.4 %copy-start.5 = (bf16[512,256]{1,0:T(8,128)(2,1)S(1)}, bf16[512,256]{1,0:T(8,128)(2,1)}, u32[]{:S(2)}) copy-start(bf16[512,256]{1,0:T(8,128)(2,1)} %param.7) | copy-start | bytes 786436
  124.1 17.6 %copy-start.7 = (bf16[2,512]{1,0:T(2,128)(2,1)S(1)}, bf16[2,512]{1,0:T(2,128)(2,1)}, u32[]{:S(2)}) copy-start(bf16[2,512]{1,0:T(2,128)(2,1)} %param.13) | copy-start | bytes 6148
  140.9 71.2 %all-gather.37.cloned.1.call-start = ((), (), s32[]{:S(2)}) async-start(), calls=%async_computation.8 | async-start | bytes 2621440 | tf_op jit(solution)/shard_map/all_gather | solution.py:41
  141.5 101.4 %all-gather.25.cloned.1.call-start = ((), (), s32[]{:S(2)}) async-start(), calls=%async_computation.2 | async-start | bytes 2359296 | tf_op jit(solution)/shard_map/all_gather | solution.py:44
  190.9 88.4 %all-gather.35.cloned.1.call-start = ((), (), s32[]{:S(2)}) async-start(), calls=%async_computation.7 | async-start | bytes 2621440 | tf_op jit(solution)/shard_map/all_gather | solution.py:40
  191.7 124.6 %all-gather.39.cloned.1.call-start = ((), (), s32[]{:S(2)}) async-start(), calls=%async_computation.9 | async-start | bytes 2621440 | tf_op jit(solution)/shard_map/all_gather | solution.py:42
  192.4 149.2 %all-gather.27.cloned.1.call-start = ((), (), s32[]{:S(2)}) async-start(), calls=%async_computation.3 | async-start | bytes 1179648 | tf_op jit(solution)/shard_map/all_gather | solution.py:71
  242.9 36.4 %copy-start.2 = (bf16[4096,256]{0,1:T(8,128)(2,1)S(1)}, bf16[4096,256]{0,1:T(8,128)(2,1)}, u32[]{:S(2)}) copy-start(bf16[4096,256]{0,1:T(8,128)(2,1)} %all-gather.25.cloned.1.call-done) | copy-start | bytes 6291460
  281.7 5.9 %collective-permute-start.3 = (bf16[256,15]{0,1:T(8,128)(2,1)S(1)}, bf16[256,15]{0,1:T(8,128)(2,1)S(1)}, u32[]{:S(2)}, u32[]{:S(2)}) collective-permute-start(bf16[256,15]{0,1:T(8,128)(2,1)S(1)} %get-tuple-element.20), channel_id=1, source_target_pairs={{8,0},{16,8},{24,16},{9,1},{17,9},{25,17},{10,2},{18,10},{26,18},{... | collective-permute-start | bytes 23048 | tf_op jit(solution)/shard_map/ppermute | solution.py:21
  283.0 5.9 %collective-permute-start.2 = (bf16[256,15]{0,1:T(8,128)(2,1)S(1)}, bf16[256,15]{0,1:T(8,128)(2,1)S(1)}, u32[]{:S(2)}, u32[]{:S(2)}) collective-permute-start(bf16[256,15]{0,1:T(8,128)(2,1)S(1)} %get-tuple-element.19), channel_id=1, source_target_pairs={{0,8},{8,16},{16,24},{1,9},{9,17},{17,25},{2,10},{10,18},{18,26},{... | collective-permute-start | bytes 23048 | tf_op jit(solution)/shard_map/ppermute | solution.py:19
  305.7 49.5 %copy-start = (bf16[512,256]{0,1:T(8,128)(2,1)S(1)}, bf16[512,256]{0,1:T(8,128)(2,1)}, u32[]{:S(2)}) copy-start(bf16[512,256]{0,1:T(8,128)(2,1)} %fusion.66) | copy-start | bytes 786436
Sparse Core Ops, SparseCore 0:
  9.2 37.8 all-gather.30
  48.7 29.1 all-gather.20
  79.7 34.5 all-gather.28
  116.0 35.0 all-gather.32
  152.5 23.8 all-gather.22
  178.2 33.9 all-gather.36
  213.7 29.1 all-gather.24
  244.8 34.5 all-gather.34
  281.2 35.0 all-gather.38
  317.7 23.8 all-gather.26
